TPU v7x, 256 devices: a 4x2x16 block of a 4x16x16 slice. The times are simulated.
256 devices in a mesh: grp: 2 (over y), fs: 16 (over z), tp: 8 (over x, core).
Axes of the slice: x: 4, y: 2, z: 16, core: 2. Of those that a mesh axis runs over, the one named last changes fastest.
The devices are a block of a 4x16x16 slice.
Arguments:
- tokens: bfloat16 [32768, 2048], P(('grp', 'fs', 'tp')), parts along dimension 0, may hold values from -12 to 12
- norm_gain: float32 [2048], replicated, may hold values from 0.1 to 1.9
- w_in: bfloat16 [2048, 8192], P('fs', 'tp'), may hold values from -0.125 to 0.125
- w_out: bfloat16 [8192, 2048], P('tp', 'fs'), may hold values from -0.0625 to 0.0625
Outputs:
- mixed: bfloat16 [32768, 2048], P(('grp', 'fs', 'tp')), parts along dimension 0
There are 2 independent parts, one for each index of `grp`. A program takes and returns all parts, laid end to end along the dimension named above; an argument that names none is the same for every part. Nothing has to cross between parts.
All inputs are finite; a program needn't handle non-finite values.
Results may differ from a plain program's by a relative error of at most 0.012.
Values may be sent and summed in bfloat16 or wider, within the bound.
No kernel may reach another device: no remote copies, remote signals or barrier semaphores. Data moves between devices by JAX's collectives and lax.ppermute only.
A program may use at most 64 MiB of HBM per device.

v0:
```python
import jax
import jax.numpy as jnp
from jax import lax
from jax.sharding import PartitionSpec as P

EPS = 1e-06


def from_everyone(shard, axis):
    copies = jnp.broadcast_to(shard, (lax.axis_size(axis), *shard.shape))
    return lax.all_to_all(copies, axis, split_axis=0, concat_axis=0, tiled=True)


def joined_along(parts, dim):
    parts = jnp.moveaxis(parts, 0, dim)
    shape = parts.shape
    return parts.reshape(*shape[:dim], shape[dim] * shape[dim + 1], *shape[dim + 2 :])


def collect(shard, axis, dim):
    parts = from_everyone(shard, axis)
    return joined_along(parts, dim)


def local(tokens, norm_gain, w_in, w_out):
    xf = tokens.astype(jnp.float32)
    scale = lax.rsqrt(jnp.mean(xf * xf, axis=-1, keepdims=True) + EPS)
    normed = (xf * scale * norm_gain).astype(jnp.bfloat16)
    whole_in = lax.all_gather(w_in, "fs", axis=0, tiled=True)
    pre = jnp.dot(collect(normed, "tp", 0), whole_in, preferred_element_type=jnp.float32)
    hidden = jnp.square(jax.nn.relu(pre)).astype(jnp.bfloat16)
    whole_out = lax.all_gather(w_out, "fs", axis=1, tiled=True)
    summed = lax.psum_scatter(
        jnp.dot(hidden, whole_out, preferred_element_type=jnp.float32).astype(jnp.bfloat16),
        "tp",
        scatter_dimension=0,
        tiled=True,
    ).astype(jnp.float32)
    return (xf + summed).astype(jnp.bfloat16)


def solution(mesh):
    in_specs = (P(("grp", "fs", "tp"), None), P(), P("fs", "tp"), P("tp", "fs"))
    out_specs = P(("grp", "fs", "tp"), None)
    return jax.shard_map(local, mesh=mesh, in_specs=in_specs, out_specs=out_specs, check_vma=False)
```

profile of v0, /device:TPU:40, one launch (start us, length us, event | category | flops | bytes accessed | tf_op | source)
XLA Modules:
  0.0 253.1 jit_solution(16195759570042781914)
XLA Ops:
  6.5 0.0 all-gather.3.cloned.1.call-start
  6.6 0.7 all-gather.3.cloned.1.call-update
  7.3 0.1 all-gather.5.cloned.1.call-start
  7.4 0.7 all-gather.5.cloned.1.call-update
  8.1 0.1 reduce-scatter.2.cloned.1.call-start
  8.2 1.2 fusion
  9.4 1.2 fusion.2
  10.7 0.5 broadcast_in_dim.2
  11.2 54.2 %all_to_all.5 = bf16[8,128,2048]{2,1,0:T(8,128)(2,1)} all-to-all(bf16[8,128,2048]{2,1,0:T(8,128)(2,1)S(1)} %broadcast_in_dim.2), channel_id=1, replica_groups=mesh['grp'=2,'fs'=16,'tp'=8] {'tp'}, dimensions={0} | all-to-all | bytes 8388608 | tf_op jit(solution)/shard_map/all_to_all | solution.py:11
  65.4 33.0 %all-gather.3.cloned.1.call-done = bf16[2048,1024]{1,0:T(8,128)(2,1)} async-done(((bf16[128,1024]{1,0:T(8,128)(2,1)}), bf16[2048,1024]{1,0:T(8,128)(2,1)}) %all-gather.3.cloned.1.call-update) | async-done | bytes 4194320 | tf_op jit(solution)/shard_map/all_gather | solution.py:29
  98.3 91.3 %all-gather.5.cloned.1.call-done = bf16[1024,2048]{1,0:T(8,128)(2,1)} async-done(((bf16[1024,128]{1,0:T(8,128)(2,1)}), bf16[1024,2048]{1,0:T(8,128)(2,1)}) %all-gather.5.cloned.1.call-update) | async-done | bytes 4194320 | tf_op jit(solution)/shard_map/all_gather | solution.py:32
  189.6 14.4 %convolution_convert_fusion = bf16[1024,2048]{1,0:T(8,128)(2,1)} fusion(bf16[1024,2048]{1,0:T(8,128)(2,1)} %all-gather.5.cloned.1.call-done, bf16[1024,2048]{1,0:T(8,128)(2,1)} %bitcast.4, bf16[2048,1024]{1,0:T(8,128)(2,1)} %all-gather.3.cloned.1.call-done), kind=kOutput, calls=%fused_computation.1 | convolution fusion | flops 8595177472 | bytes 16777216 | tf_op jit(solution)/shard_map/dot_general | solution.py:34
  204.0 0.0 copy-start
  204.0 0.1 reduce-scatter.2.cloned.1.call-update
  204.1 40.5 %reduce-scatter.2.cloned.1.call-done = bf16[128,2048]{1,0:T(8,128)(2,1)} async-done(((bf16[1024,2048]{1,0:T(8,128)(2,1)}), bf16[128,2048]{1,0:T(8,128)(2,1)}) %reduce-scatter.2.cloned.1.call-update) | async-done | bytes 524304 | tf_op jit(solution)/shard_map/reduce_scatter | solution.py:33
  244.5 0.0 copy-done
  244.5 2.0 fusion.3
  (1 shorter events, 0.0 us)
Async XLA Ops:
  6.5 91.8 %all-gather.3.cloned.1.call-start = ((), (), s32[]{:S(2)}) async-start(), calls=%async_computation.2 | async-start | bytes 4456448 | tf_op jit(solution)/shard_map/all_gather | solution.py:29
  7.3 182.3 %all-gather.5.cloned.1.call-start = ((), (), s32[]{:S(2)}) async-start(), calls=%async_computation.3 | async-start | bytes 4456448 | tf_op jit(solution)/shard_map/all_gather | solution.py:32
  8.1 236.4 %reduce-scatter.2.cloned.1.call-start = ((), (), s32[]{:S(2)}) async-start(), calls=%async_computation.4 | async-start | bytes 4718592 | tf_op jit(solution)/shard_map/reduce_scatter | solution.py:33
  204.0 40.6 %copy-start = (bf16[128,2048]{1,0:T(8,128)(2,1)S(1)}, bf16[128,2048]{1,0:T(8,128)(2,1)}, u32[]{:S(2)}) copy-start(bf16[128,2048]{1,0:T(8,128)(2,1)} %param.4) | copy-start | bytes 1572868
Sparse Core Ops, SparseCore 0:
  9.1 89.1 all-gather.2
  100.1 89.5 all-gather.4
  204.2 40.3 reduce-scatter.1
where the time goes:
time: 253 us
  waiting for transfers between devices  166 us (66%)
  blocking collectives  54.2 us (21%)
  matrix products  14.4 us (6%)
  between operations  13.1 us (5%)
  other arithmetic  4.44 us (2%)
    all_gather x1, waiting for transfers between devices, local(): whole_out = lax.all_gather(w_out, 'fs', axis=1, tiled=True)  91.3 us
    all_to_all x1, blocking collectives, from_everyone(): return lax.all_to_all(copies, axis, split_axis=0, concat_axis=0, tiled=True)  54.2 us
    reduce_scatter x1, waiting for transfers between devices, local(): lax.psum_scatter(jnp.dot(hidden, whole_out, preferred_element_type=jnp.fl...  40.5 us
    all_gather x1, waiting for transfers between devices, local(): whole_in = lax.all_gather(w_in, 'fs', axis=0, tiled=True)  33 us
    dot_general x1, matrix products, local(): jnp.dot(hidden, whole_out, preferred_element_type=jnp.float32)  14.4 us
  transfers between devices with their start and end apart: 3, of which 3 were waited for; matrix products, arithmetic and copies ran while one was open for 1% of the time, Pallas kernels for 0%

commit v1 on v0

--- a/solution.py
+++ b/solution.py
@@ -29,7 +29,10 @@
     whole_in = lax.all_gather(w_in, "fs", axis=0, tiled=True)
     pre = jnp.dot(collect(normed, "tp", 0), whole_in, preferred_element_type=jnp.float32)
     hidden = jnp.square(jax.nn.relu(pre)).astype(jnp.bfloat16)
-    whole_out = lax.all_gather(w_out, "fs", axis=1, tiled=True)
+    size = lax.axis_size("fs")
+    blocks = jnp.stack([w_out for _ in range(size)])
+    blocks = lax.all_to_all(blocks, "fs", split_axis=0, concat_axis=0)
+    whole_out = jnp.concatenate(blocks, axis=1)
     summed = lax.psum_scatter(
         jnp.dot(hidden, whole_out, preferred_element_type=jnp.float32).astype(jnp.bfloat16),
         "tp",

time: 253 us -> 384 us (1.52)
  waiting for transfers between devices: 166 us -> 318 us
  blocking collectives: 54.2 us -> 0 us
  starting transfers between devices: 0.13 us -> 29 us
  local copies, waits for them, and re-layouts: 0.52 us -> 5.13 us
    all_gather x1, waiting for transfers between devices: 33 us -> 227 us  [local(): whole_in = lax.all_gather(w_in, 'fs', axis=0, tiled=True)]
    all_gather x1 -> x0, waiting for transfers between devices: 91.3 us -> none  [local(): whole_out = lax.all_gather(w_out, 'fs', axis=1, tiled=True)]
    all_to_all x1 -> x0, blocking collectives: 54.2 us -> none  [from_everyone(): return lax.all_to_all(copies, axis, split_axis=0, concat_axis=0, tiled=True)]
    all_to_all x0 -> x2, waiting for transfers between devices: none -> 49.4 us  [the longest x1 49.4 us: from_everyone(): return lax.all_to_all(copies, axis, split_axis=0, concat_axis=0, tiled=True)]
    all_to_all x0 -> x2, starting transfers between devices: none -> 28.8 us  [the longest x1 24 us: local(): blocks = lax.all_to_all(blocks, 'fs', split_axis=0, concat_axis=0)]
  transfers between devices with their start and end apart: 3 -> 4, of which waited for: 3 -> 3; matrix products, arithmetic and copies ran while one was open for 1% -> 0% of each run, Pallas kernels for 0% -> 0%
where the time goes in v1:
time: 384 us
  waiting for transfers between devices  318 us (83%)
  starting transfers between devices  29 us (8%)
  matrix products  14.4 us (4%)
  between operations  13.5 us (4%)
  local copies, waits for them, and re-layouts  5.13 us (1%)
  other arithmetic  4.44 us (1%)
    all_gather x1, waiting for transfers between devices, local(): whole_in = lax.all_gather(w_in, 'fs', axis=0, tiled=True)  227 us
    all_to_all x1, waiting for transfers between devices, from_everyone(): return lax.all_to_all(copies, axis, split_axis=0, concat_axis=0, tiled=True)  49.4 us
    reduce_scatter x1, waiting for transfers between devices, local(): lax.psum_scatter(jnp.dot(hidden, whole_out, preferred_element_type=jnp.fl...  40.1 us
    all_to_all x1, starting transfers between devices, local(): blocks = lax.all_to_all(blocks, 'fs', split_axis=0, concat_axis=0)  24 us
    dot_general x1, matrix products, local(): jnp.dot(hidden, whole_out, preferred_element_type=jnp.float32)  14.4 us
  transfers between devices with their start and end apart: 4, of which 3 were waited for; matrix products, arithmetic and copies ran while one was open for 0% of the time, Pallas kernels for 0%

profile of v1, /device:TPU:40, one launch (start us, length us, event | category | flops | bytes accessed | tf_op | source)
XLA Modules:
  0.0 383.9 jit_solution(15606499029884411505)
XLA Ops:
  6.5 1.2 fusion
  7.8 1.2 fusion.2
  9.0 2.5 broadcast_in_dim.2
  11.5 0.0 copy-start.1
  11.5 4.9 %all-to-all-start = ((bf16[8,128,2048]{2,1,0:T(8,128)(2,1)}), bf16[8,128,2048]{2,1,0:T(8,128)(2,1)}, u32[]{:S(2)}, u32[]{:S(2)}) async-start(bf16[8,128,2048]{2,1,0:T(8,128)(2,1)} %broadcast_in_dim.2), calls=%async_computation | async-start | bytes 8388608 | tf_op jit(solution)/shard_map/all_to_all | solution.py:11
  16.4 0.0 copy-done.1
  16.4 0.1 copy.5
  16.6 49.4 %all-to-all-done = bf16[8,128,2048]{2,1,0:T(8,128)(2,1)} async-done(((bf16[8,128,2048]{2,1,0:T(8,128)(2,1)}), bf16[8,128,2048]{2,1,0:T(8,128)(2,1)}, u32[]{:S(2)}, u32[]{:S(2)}) %all-to-all-start) | async-done | bytes 4194336 | tf_op jit(solution)/shard_map/all_to_all | solution.py:11
  66.0 2.5 stack.2
  68.5 24.0 %all-to-all-start.1 = ((bf16[16,1024,128]{1,2,0:T(8,128)(2,1)}), bf16[16,1024,128]{1,2,0:T(8,128)(2,1)}, u32[]{:S(2)}, u32[]{:S(2)}) async-start(bf16[16,1024,128]{1,2,0:T(8,128)(2,1)} %stack.2), calls=%async_computation.1 | async-start | bytes 8388608 | tf_op jit(solution)/shard_map/all_to_all | solution.py:34
  92.5 0.1 all-gather.2.cloned.1.call-start
  92.5 0.7 all-gather.2.cloned.1.call-update
  93.3 0.1 reduce-scatter.2.cloned.1.call-start
  93.3 227.2 %all-gather.2.cloned.1.call-done = bf16[2048,1024]{1,0:T(8,128)(2,1)} async-done(((bf16[128,1024]{1,0:T(8,128)(2,1)}), bf16[2048,1024]{1,0:T(8,128)(2,1)}) %all-gather.2.cloned.1.call-update) | async-done | bytes 4194320 | tf_op jit(solution)/shard_map/all_gather | solution.py:29
  320.5 0.0 all-to-all-done.1
  320.5 14.4 %convolution_convert_fusion = bf16[1024,2048]{1,0:T(8,128)(2,1)} fusion(bf16[1024,2048]{0,1:T(8,128)(2,1)} %bitcast.2, bf16[1024,2048]{1,0:T(8,128)(2,1)} %bitcast, bf16[2048,1024]{1,0:T(8,128)(2,1)} %all-gather.2.cloned.1.call-done), kind=kOutput, calls=%fused_computation.1 | convolution fusion | flops 8595177472 | bytes 16777216 | tf_op jit(solution)/shard_map/dot_general | solution.py:37
  334.9 0.0 copy-start
  334.9 0.1 reduce-scatter.2.cloned.1.call-update
  335.0 40.1 %reduce-scatter.2.cloned.1.call-done = bf16[128,2048]{1,0:T(8,128)(2,1)} async-done(((bf16[1024,2048]{1,0:T(8,128)(2,1)}), bf16[128,2048]{1,0:T(8,128)(2,1)}) %reduce-scatter.2.cloned.1.call-update) | async-done | bytes 524304 | tf_op jit(solution)/shard_map/reduce_scatter | solution.py:36
  375.1 0.0 copy-done
  375.1 2.0 fusion.3
  (1 shorter events, 0.0 us)
Async XLA Ops:
  11.5 4.9 %copy-start.1 = (bf16[1024,128]{1,0:T(8,128)(2,1)S(1)}, bf16[1024,128]{1,0:T(8,128)(2,1)}, u32[]{:S(2)}) copy-start(bf16[1024,128]{1,0:T(8,128)(2,1)} %param.7) | copy-start | bytes 786436
  11.5 54.5 %all-to-all-start = ((bf16[8,128,2048]{2,1,0:T(8,128)(2,1)}), bf16[8,128,2048]{2,1,0:T(8,128)(2,1)}, u32[]{:S(2)}, u32[]{:S(2)}) async-start(bf16[8,128,2048]{2,1,0:T(8,128)(2,1)} %broadcast_in_dim.2), calls=%async_computation | async-start | bytes 8388608 | tf_op jit(solution)/shard_map/all_to_all | solution.py:11
  68.5 252.1 %all-to-all-start.1 = ((bf16[16,1024,128]{1,2,0:T(8,128)(2,1)}), bf16[16,1024,128]{1,2,0:T(8,128)(2,1)}, u32[]{:S(2)}, u32[]{:S(2)}) async-start(bf16[16,1024,128]{1,2,0:T(8,128)(2,1)} %stack.2), calls=%async_computation.1 | async-start | bytes 8388608 | tf_op jit(solution)/shard_map/all_to_all | solution.py:34
  92.5 228.1 %all-gather.2.cloned.1.call-start = ((), (), s32[]{:S(2)}) async-start(), calls=%async_computation.3 | async-start | bytes 4456448 | tf_op jit(solution)/shard_map/all_gather | solution.py:29
  93.3 281.8 %reduce-scatter.2.cloned.1.call-start = ((), (), s32[]{:S(2)}) async-start(), calls=%async_computation.4 | async-start | bytes 4718592 | tf_op jit(solution)/shard_map/reduce_scatter | solution.py:36
  334.9 40.2 %copy-start = (bf16[128,2048]{1,0:T(8,128)(2,1)S(1)}, bf16[128,2048]{1,0:T(8,128)(2,1)}, u32[]{:S(2)}) copy-start(bf16[128,2048]{1,0:T(8,128)(2,1)} %param.4) | copy-start | bytes 1572868
Sparse Core Ops, SparseCore 0:
  95.1 225.3 all-gather.1
  335.1 39.9 reduce-scatter.1
